TPU v7x, 256 devices: a whole 4x4x8 slice. The times are simulated.
256 devices in a mesh: ra: 32 (over z, y), cb: 8 (over x, core).
Axes of the slice: x: 4, y: 4, z: 8, core: 2. Of those that a mesh axis runs over, the one named last changes fastest.
Arguments:
- stream: bfloat16 [64, 1024], P(None, 'ra'), may hold values from -24 to 24, as said below
- gain_first: float32 [1024], P('ra'), may hold values from 0.5 to 1.5
- up_first: float32 [1024, 4096], P('ra', 'cb'), may hold values from -0.1875 to 0.1875
- down_first: float32 [4096, 1024], P('cb', 'ra'), may hold values from -0.09375 to 0.09375
- gain_second: float32 [1024], P('ra'), may hold values from 0.5 to 1.5
- up_second: float32 [1024, 4096], P('ra', 'cb'), may hold values from -0.1875 to 0.1875
- down_second: float32 [4096, 1024], P('cb', 'ra'), may hold values from -0.09375 to 0.09375
Outputs:
- read: bfloat16 [64, 1024], P(None, 'ra')
Inputs may be any that keep to these rules, and one draw needn't show every extreme that they name: stream is of order one, and in each token one aligned block of 32 features is four times larger than the rest.
All inputs are finite; a program needn't handle non-finite values.
Results may differ from a plain program's by a relative error of at most 0.025.
Values may be sent and summed in bfloat16 or wider, within the bound.
A program may use at most 64 MiB of HBM per device.

v0:
```python
import jax
import jax.numpy as jnp
from jax import lax
from jax.sharding import Mesh
from jax.sharding import PartitionSpec as P

D = 1024
RA = ("ra_0", "ra_1")
EPS = 1e-06
RESIDUAL = 0.25


def by_axis(array, axes):
    for axis in axes:
        array = lax.psum(array, axis)
    return array


def total_of_pieces(array, axis):
    pieces = lax.all_gather(array, axis)
    return pieces.sum(axis=0)


def over_pieces(array, axis):
    return lax.all_gather(array, axis).astype(jnp.float32).sum(0)


def sublayer(stream, norm_gain, w_up, w_down):
    floated = stream.astype(jnp.float32)
    own_squares = jnp.sum(floated * floated, axis=1, keepdims=True)
    squares = by_axis(own_squares, RA)
    factor = lax.rsqrt(squares / D + EPS)
    normed = (floated * factor * norm_gain.astype(jnp.float32)[None, :]).astype(jnp.bfloat16)
    up_bf = w_up.astype(jnp.bfloat16)
    down_bf = w_down.astype(jnp.bfloat16)
    partial_value = jnp.dot(normed, up_bf, preferred_element_type=jnp.float32)
    preact = total_of_pieces(partial_value, RA)
    activated = jnp.square(jax.nn.relu(preact)).astype(jnp.bfloat16)
    down_part = jnp.dot(activated, down_bf, preferred_element_type=jnp.float32)
    branch = over_pieces(down_part.astype(jnp.bfloat16), "cb").astype(jnp.float32)
    return (RESIDUAL * floated + branch).astype(jnp.bfloat16)


def local(stream, gain_first, up_first, down_first, gain_second, up_second, down_second):
    middle = sublayer(stream, gain_first, up_first, down_first)
    return sublayer(middle, gain_second, up_second, down_second)


def solution(mesh):
    torus = Mesh(mesh.devices.reshape(8, 4, mesh.shape["cb"]), ("ra_0", "ra_1", "cb"))
    in_specs = (P(None, RA), P(RA), P(RA, "cb"), P("cb", RA), P(RA), P(RA, "cb"), P("cb", RA))
    out_specs = P(None, RA)
    return jax.shard_map(local, mesh=torus, in_specs=in_specs, out_specs=out_specs, check_vma=False)
```

profile of v0, /device:TPU:1, one launch (start us, length us, event | category | flops | bytes accessed | tf_op | source)
XLA Modules:
  0.0 262.2 jit_solution(6546073855465038196)
XLA Ops:
  6.5 0.0 all-gather.9.cloned.1.call-start
  6.6 0.8 fusion.12
  7.3 17.3 %psum.28 = f32[64,1]{0,1:T(1,128)S(1)} all-reduce(f32[64,1]{0,1:T(1,128)S(1)} %bitcast.15), channel_id=1, replica_groups=mesh['ra_0'=8,'ra_1'=4,'cb'=8] {'ra_0'}, use_global_device_ids=true, to_apply=%region_1.0 | all-reduce | flops 64 | bytes 512 | tf_op jit(solution)/shard_map/psum | solution.py:15
  24.6 8.7 %psum.29 = f32[64,1]{0,1:T(1,128)S(1)} all-reduce(f32[64,1]{0,1:T(1,128)S(1)} %psum.28), channel_id=1, replica_groups=mesh['ra_0'=8,'ra_1'=4,'cb'=8] {'ra_1'}, use_global_device_ids=true, to_apply=%region_2.0 | all-reduce | flops 64 | bytes 512 | tf_op jit(solution)/shard_map/psum | solution.py:15
  33.3 1.8 fusion.8
  35.1 0.0 all-gather.9.cloned.1.call-update
  35.1 0.0 all-gather.11.cloned.1.call-start
  35.2 79.7 %all-gather.9.cloned.1.call-done = f32[2048,512]{1,0:T(8,128)} async-done(((f32[64,512]{1,0:T(8,128)}), f32[2048,512]{1,0:T(8,128)}) %all-gather.9.cloned.1.call-update) | async-done | bytes 4194320 | tf_op jit(solution)/shard_map/all_gather | solution.py:20
  114.9 2.6 reduce_sum.55
  117.5 0.0 copy-done.1
  117.5 0.1 fusion
  117.6 17.1 %all-gather.4 = bf16[8,64,32]{1,2,0:T(8,128)(2,1)S(1)} all-gather(bf16[1,64,32]{1,2,0:T(8,128)(2,1)S(1)} %fusion), channel_id=3, replica_groups=mesh['ra_0'=8,'ra_1'=4,'cb'=8] {'cb'}, dimensions={0}, use_global_device_ids=true | all-gather | bytes 36864 | tf_op jit(solution)/shard_map/all_gather | solution.py:25
  134.7 0.0 copy-done
  134.8 12.3 %psum.30 = f32[64,1]{0,1:T(1,128)S(1)} all-reduce(f32[64,1]{0,1:T(1,128)S(1)} %bitcast.14), channel_id=1, replica_groups=mesh['ra_0'=8,'ra_1'=4,'cb'=8] {'ra_0'}, use_global_device_ids=true, to_apply=%region_6.7 | all-reduce | flops 64 | bytes 512 | tf_op jit(solution)/shard_map/psum | solution.py:15
  147.1 6.5 %psum.31 = f32[64,1]{0,1:T(1,128)S(1)} all-reduce(f32[64,1]{0,1:T(1,128)S(1)} %psum.30), channel_id=1, replica_groups=mesh['ra_0'=8,'ra_1'=4,'cb'=8] {'ra_1'}, use_global_device_ids=true, to_apply=%region_7.8 | all-reduce | flops 64 | bytes 512 | tf_op jit(solution)/shard_map/psum | solution.py:15
  153.6 0.0 copy-done.2
  153.7 0.0 copy-done.4
  153.7 0.9 fusion.5
  154.6 0.0 all-gather.11.cloned.1.call-update
  154.6 80.4 %all-gather.11.cloned.1.call-done = f32[2048,512]{1,0:T(8,128)} async-done(((f32[64,512]{1,0:T(8,128)}), f32[2048,512]{1,0:T(8,128)}) %all-gather.11.cloned.1.call-update) | async-done | bytes 4194320 | tf_op jit(solution)/shard_map/all_gather | solution.py:20
  234.9 2.5 reduce_sum.58
  237.5 0.1 fusion.1
  237.6 17.1 %all-gather.5 = bf16[8,64,32]{1,2,0:T(8,128)(2,1)S(1)} all-gather(bf16[1,64,32]{1,2,0:T(8,128)(2,1)S(1)} %fusion.1), channel_id=5, replica_groups=mesh['ra_0'=8,'ra_1'=4,'cb'=8] {'cb'}, dimensions={0}, use_global_device_ids=true | all-gather | bytes 36864 | tf_op jit(solution)/shard_map/all_gather | solution.py:25
  254.7 0.6 fusion.16
  (11 shorter events, 0.1 us)
Async XLA Ops:
  6.5 128.2 %copy-start = (bf16[64,32]{0,1:T(8,128)(2,1)S(1)}, bf16[64,32]{0,1:T(8,128)(2,1)}, u32[]{:S(2)}) copy-start(bf16[64,32]{0,1:T(8,128)(2,1)} %param.7) | copy-start | bytes 12292
  6.5 111.0 %copy-start.1 = (f32[512,32]{0,1:T(8,128)S(1)}, f32[512,32]{0,1:T(8,128)}, u32[]{:S(2)}) copy-start(f32[512,32]{0,1:T(8,128)} %param.10) | copy-start | bytes 196612
  6.5 147.1 %copy-start.2 = (f32[32,512]{1,0:T(8,128)S(1)}, f32[32,512]{1,0:T(8,128)}, u32[]{:S(2)}) copy-start(f32[32,512]{1,0:T(8,128)} %param.12) | copy-start | bytes 196612
  6.5 147.1 %copy-start.4 = (f32[32]{0:T(128)S(1)}, f32[32]{0:T(128)}, u32[]{:S(2)}) copy-start(f32[32]{0:T(128)} %param.11) | copy-start | bytes 388
  6.5 108.4 %all-gather.9.cloned.1.call-start = ((), (), s32[]{:S(2)}) async-start(), calls=%async_computation | async-start | bytes 4325376 | tf_op jit(solution)/shard_map/all_gather | solution.py:20
  35.1 199.8 %all-gather.11.cloned.1.call-start = ((), (), s32[]{:S(2)}) async-start(), calls=%async_computation.1 | async-start | bytes 4325376 | tf_op jit(solution)/shard_map/all_gather | solution.py:20
  114.9 122.5 %copy-start.3 = (f32[512,32]{0,1:T(8,128)S(1)}, f32[512,32]{0,1:T(8,128)}, u32[]{:S(2)}) copy-start(f32[512,32]{0,1:T(8,128)} %param.13) | copy-start | bytes 196612
Sparse Core Ops, SparseCore 0:
  35.3 79.6 all-gather.8
  154.7 80.1 all-gather.10
where the time goes:
time: 262 us
  waiting for transfers between devices  160 us (61%)
  blocking collectives  79 us (30%)
  between operations  13.4 us (5%)
  other arithmetic  6.52 us (2%)
  matrix products  2.95 us (1%)
    all_gather x2, waiting for transfers between devices, total_of_pieces(): pieces = lax.all_gather(array, axis)  160 us
    psum x4, blocking collectives, by_axis(): array = lax.psum(array, axis)  44.9 us
    all_gather x2, blocking collectives, over_pieces(): return lax.all_gather(array, axis).astype(jnp.float32).sum(0)  34.2 us
  transfers between devices with their start and end apart: 2, of which 2 were waited for; matrix products, arithmetic and copies ran while one was open for 0% of the time, Pallas kernels for 0%

commit v1 on v0

--- a/solution.py
+++ b/solution.py
@@ -8,11 +8,12 @@
 RA = ("ra_0", "ra_1")
 EPS = 1e-06
 RESIDUAL = 0.25
+handle_turns = lambda inner_x, axis_id: lax.all_gather(inner_x, axis_id).sum(axis=0)
 
 
 def by_axis(array, axes):
     for axis in axes:
-        array = lax.psum(array, axis)
+        array = handle_turns(array, axis)
     return array
 
 

time: 262 us -> 268 us (1.023)
  local copies, waits for them, and re-layouts: 0.02 us -> 3.88 us
    psum x4 -> x0, blocking collectives: 44.9 us -> none  [by_axis(): array = lax.psum(array, axis)]
    unnamed x0 -> x4, blocking collectives: none -> 44.8 us
    unnamed x10 -> x20, local copies, waits for them, and re-layouts: 0.02 us -> 3.55 us
where the time goes in v1:
time: 268 us; the launch traced here: 267 us
  waiting for transfers between devices  160 us (60%)
  blocking collectives  79 us (29%)
  between operations  14.8 us (6%)
  other arithmetic  6.61 us (2%)
  local copies, waits for them, and re-layouts  3.88 us (1%)
  matrix products  2.95 us (1%)
    all_gather x2, waiting for transfers between devices, total_of_pieces(): pieces = lax.all_gather(array, axis)  160 us
    unnamed x4, blocking collectives  44.8 us
    all_gather x2, blocking collectives, over_pieces(): return lax.all_gather(array, axis).astype(jnp.float32).sum(0)  34.2 us
  transfers between devices with their start and end apart: 2, of which 2 were waited for; matrix products, arithmetic and copies ran while one was open for 0% of the time, Pallas kernels for 0%

profile of v1, /device:TPU:1, one launch (start us, length us, event | category | flops | bytes accessed | tf_op | source)
XLA Modules:
  0.0 267.4 jit_solution(8511208917221614598)
XLA Ops:
  6.6 0.8 fusion.12
  7.3 1.3 dynamic-slice
  9.3 0.2 dynamic-update-slice
  9.5 17.3 %all-reduce = f32[512]{0:T(512)S(1)} all-reduce(f32[512]{0:T(512)S(1)} %dynamic-update-slice), channel_id=2, replica_groups=mesh['ra_0'=8,'ra_1'=4,'cb'=8] {'ra_0'}, use_global_device_ids=true, to_apply=%add | all-reduce | flops 512 | bytes 4096
  26.9 1.3 dynamic-slice.1
  28.8 0.2 dynamic-update-slice.1
  29.0 8.7 %all-reduce.1 = f32[256]{0:T(256)S(1)} all-reduce(f32[256]{0:T(256)S(1)} %dynamic-update-slice.1), channel_id=3, replica_groups=mesh['ra_0'=8,'ra_1'=4,'cb'=8] {'ra_1'}, use_global_device_ids=true, to_apply=%add.1 | all-reduce | flops 256 | bytes 2048
  37.7 0.1 reshape.25
  37.9 1.8 fusion.8
  39.7 79.7 %all-gather.13.cloned.1.call-done = f32[2048,512]{1,0:T(8,128)} async-done(((f32[64,512]{1,0:T(8,128)}), f32[2048,512]{1,0:T(8,128)}) %all-gather.13.cloned.1.call-update) | async-done | bytes 4194320 | tf_op jit(solution)/shard_map/all_gather | solution.py:21
  119.4 2.6 reduce_sum.93
  122.0 0.1 fusion
  122.1 17.1 %all-gather.8 = bf16[8,64,32]{1,2,0:T(8,128)(2,1)S(1)} all-gather(bf16[1,64,32]{1,2,0:T(8,128)(2,1)S(1)} %fusion), channel_id=5, replica_groups=mesh['ra_0'=8,'ra_1'=4,'cb'=8] {'cb'}, dimensions={0}, use_global_device_ids=true | all-gather | bytes 36864 | tf_op jit(solution)/shard_map/all_gather | solution.py:26
  139.3 0.2 dynamic-update-slice.2
  139.5 12.3 %all-reduce.2 = f32[512]{0:T(512)S(1)} all-reduce(f32[512]{0:T(512)S(1)} %dynamic-update-slice.2), channel_id=6, replica_groups=mesh['ra_0'=8,'ra_1'=4,'cb'=8] {'ra_0'}, use_global_device_ids=true, to_apply=%add.2 | all-reduce | flops 512 | bytes 4096
  152.0 0.2 dynamic-update-slice.3
  152.2 6.5 %all-reduce.3 = f32[256]{0:T(256)S(1)} all-reduce(f32[256]{0:T(256)S(1)} %dynamic-update-slice.3), channel_id=7, replica_groups=mesh['ra_0'=8,'ra_1'=4,'cb'=8] {'ra_1'}, use_global_device_ids=true, to_apply=%add.3 | all-reduce | flops 256 | bytes 2048
  158.7 0.1 reshape.29
  158.8 0.9 fusion.5
  159.8 80.4 %all-gather.15.cloned.1.call-done = f32[2048,512]{1,0:T(8,128)} async-done(((f32[64,512]{1,0:T(8,128)}), f32[2048,512]{1,0:T(8,128)}) %all-gather.15.cloned.1.call-update) | async-done | bytes 4194320 | tf_op jit(solution)/shard_map/all_gather | solution.py:21
  240.1 2.5 reduce_sum.98
  242.7 0.1 fusion.1
  242.8 17.1 %all-gather.9 = bf16[8,64,32]{1,2,0:T(8,128)(2,1)S(1)} all-gather(bf16[1,64,32]{1,2,0:T(8,128)(2,1)S(1)} %fusion.1), channel_id=9, replica_groups=mesh['ra_0'=8,'ra_1'=4,'cb'=8] {'cb'}, dimensions={0}, use_global_device_ids=true | all-gather | bytes 36864 | tf_op jit(solution)/shard_map/all_gather | solution.py:26
  259.9 0.6 fusion.16
  (29 shorter events, 0.5 us)
Async XLA Ops:
  6.5 132.7 %copy-start = (bf16[64,32]{0,1:T(8,128)(2,1)S(1)}, bf16[64,32]{0,1:T(8,128)(2,1)}, u32[]{:S(2)}) copy-start(bf16[64,32]{0,1:T(8,128)(2,1)} %param.7) | copy-start | bytes 12292
  6.5 115.5 %copy-start.1 = (f32[512,32]{0,1:T(8,128)S(1)}, f32[512,32]{0,1:T(8,128)}, u32[]{:S(2)}) copy-start(f32[512,32]{0,1:T(8,128)} %param.10) | copy-start | bytes 196612
  6.5 152.3 %copy-start.4 = (f32[32]{0:T(128)S(1)}, f32[32]{0:T(128)}, u32[]{:S(2)}) copy-start(f32[32]{0:T(128)} %param.11) | copy-start | bytes 388
  6.5 152.3 %copy-start.2 = (f32[32,512]{1,0:T(8,128)S(1)}, f32[32,512]{1,0:T(8,128)}, u32[]{:S(2)}) copy-start(f32[32,512]{1,0:T(8,128)} %param.12) | copy-start | bytes 196612
  6.5 112.9 %all-gather.13.cloned.1.call-start = ((), (), s32[]{:S(2)}) async-start(), calls=%async_computation | async-start | bytes 4325376 | tf_op jit(solution)/shard_map/all_gather | solution.py:21
  39.7 200.5 %all-gather.15.cloned.1.call-start = ((), (), s32[]{:S(2)}) async-start(), calls=%async_computation.1 | async-start | bytes 4325376 | tf_op jit(solution)/shard_map/all_gather | solution.py:21
  119.4 123.2 %copy-start.3 = (f32[512,32]{0,1:T(8,128)S(1)}, f32[512,32]{0,1:T(8,128)}, u32[]{:S(2)}) copy-start(f32[512,32]{0,1:T(8,128)} %param.13) | copy-start | bytes 196612
Sparse Core Ops, SparseCore 0:
  39.8 79.6 all-gather.12
  159.9 80.1 all-gather.14
